TPU v7x, 512 devices: a 8x2x16 block of a 8x8x16 slice. The times are simulated.
512 devices in a mesh: grp: 2 (over y), sp: 32 (over z, core), tp: 8 (over x).
Axes of the slice: x: 8, y: 2, z: 16, core: 2. Of those that a mesh axis runs over, the one named last changes fastest.
The devices are a block of a 8x8x16 slice.
Arguments:
- tokens: bfloat16 [8, 4096, 4096], P('grp', 'sp'), parts along dimension 0, may hold values from -9 to 9
- w_forget: bfloat16 [4096, 4096], P('sp', 'tp'), may hold values from -0.09375 to 0.09375
- w_value: bfloat16 [4096, 4096], P('sp', 'tp'), may hold values from -0.09375 to 0.09375
- lower_bound: float32 [4096], P('tp'), may hold values from 0.25 to 1
- decay_shift: float32 [8, 4096, 32], P('grp', 'sp', 'tp'), parts along dimension 0, may hold values from -1 to 0
- queries: bfloat16 [8, 4096], P('grp', 'tp'), parts along dimension 0, may hold values from -6 to 6
- read_gain: float32 [4096], P('tp'), may hold values from 0.1 to 1.9
Outputs:
- cache_out: bfloat16 [8, 32, 16384], P('grp', 'tp', 'sp'), parts along dimension 0
- first_read: bfloat16 [8, 4096], P('grp', 'tp'), parts along dimension 0
There are 2 independent parts, one for each index of `grp`. A program takes and returns all parts, laid end to end along the dimension named above; an argument that names none is the same for every part. Nothing has to cross between parts.
All inputs are finite; a program needn't handle non-finite values.
Results may differ from a plain program's by a relative error of at most 0.01.
Values may be sent and summed in bfloat16 or wider, within the bound.
A program may use at most 128 MiB of HBM per device.

v0:
```python
import jax
import jax.numpy as jnp
from jax import lax
from jax.sharding import PartitionSpec as P

DK = 128
DV = 128


def side_by_side(arrays, axis, dim, along):
    both = jnp.concatenate(arrays, axis=along)
    whole, at, gathered = (lax.all_gather(both, axis, axis=dim, tiled=True), 0, [])
    for a in arrays:
        gathered.append(lax.slice_in_dim(whole, at, at + a.shape[along], axis=along))
        at += a.shape[along]
    return tuple(gathered)


def sent_to_all(array, axis):
    count = lax.axis_size(axis)
    return lax.all_to_all(
        jnp.broadcast_to(array[None], (count, *array.shape)), axis, 0, 0, tiled=True
    )


def joined_by_halves(pieces, combine):
    while len(jax.tree.leaves(pieces)[0]) > 1:
        pieces = jax.vmap(combine)(*(pieces[side::2] for side in (0, 1)))
    return pieces[0]


def carried_in(array, axis, combine, identity):
    count, mine = (lax.axis_size(axis), lax.axis_index(axis))
    passed = jnp.arange(count) > mine

    def kept(part, zero, own):
        part = jnp.where(
            passed.reshape(-1, *(1 for _ in own.shape)), part, jnp.asarray(zero, own.dtype)
        )
        return part[::-1]

    pieces = sent_to_all(array, axis)
    return joined_by_halves(kept(pieces, identity, array), combine)


def cut_along(array, dim, count):
    before, after = (array.shape[:dim], array.shape[dim + 1 :])
    return jnp.moveaxis(array.reshape(*before, count, -1, *after), dim, 0)


def sent_and_summed(array, axis, dim):
    blocks = cut_along(array, dim, lax.axis_size(axis))
    arrived = lax.all_to_all(blocks, axis, split_axis=0, concat_axis=0, tiled=True)
    return arrived.astype(jnp.float32).sum(axis=0)


def of_everyone(array, axis):
    everything = sent_to_all(array, axis)
    return jnp.sum(everything, axis=0)


def add_terms(earlier, later_part):
    return earlier + later_part


def shards(tokens, w_forget, w_value, lower_bound, decay_shift, queries, read_gain):
    seq_count, span_len, feat_width = tokens.shape
    tok_rows = tokens.reshape(seq_count * span_len, feat_width)
    head_local = lower_bound.shape[0] // DK
    sp_count = lax.axis_size("sp")
    own_rows = DK // sp_count
    pieces = side_by_side((w_forget, w_value), "sp", 0, 1)
    pre_gate = jnp.dot(tok_rows, pieces[0], preferred_element_type=jnp.float32)
    value_sum = jnp.dot(tok_rows, pieces[1], preferred_element_type=jnp.float32)
    values = value_sum.astype(jnp.bfloat16)
    low_bound = lower_bound[None, :]
    log_forget = jnp.logaddexp(
        jnp.log(low_bound), jnp.log1p(-low_bound) + jax.nn.log_sigmoid(pre_gate)
    )
    log_forget = log_forget.reshape(seq_count, span_len, head_local, DK) + decay_shift[..., None]
    key_gates = ((1.0 - low_bound) * jax.nn.sigmoid(-pre_gate)).reshape(
        seq_count, span_len, head_local, DK
    )
    inclusive = jnp.cumsum(log_forget, axis=1)
    totals = inclusive[:, -1]
    weighted = (key_gates * jnp.exp(totals[:, None] - inclusive)).astype(jnp.bfloat16)
    span_values = values.reshape(seq_count, span_len, head_local, DV)
    local_state = jnp.einsum(
        "sthk,sthv->shkv", weighted, span_values, preferred_element_type=jnp.float32
    )
    suffix = carried_in(totals, "sp", add_terms, jnp.zeros_like(totals))
    decayed = (jnp.exp(suffix)[..., None] * local_state).reshape(seq_count, head_local, DK * DV)
    final_state = sent_and_summed(decayed.astype(jnp.bfloat16), "sp", 2)
    cache_out = final_state.astype(jnp.bfloat16)
    query_act = jax.nn.silu(queries.astype(jnp.float32)).reshape(seq_count, head_local, DK)
    own_query = lax.dynamic_slice_in_dim(query_act, lax.axis_index("sp") * own_rows, own_rows, 2)
    partial_value = jnp.sum(
        own_query[..., None] * final_state.reshape(seq_count, head_local, own_rows, DV), axis=2
    )
    total_read = of_everyone(partial_value, "sp")
    scaled = total_read * lax.rsqrt(
        jnp.mean(total_read * total_read, axis=-1, keepdims=True) + 1e-06
    )
    first_read = (
        (scaled * read_gain.reshape(head_local, DV))
        .reshape(seq_count, head_local * DV)
        .astype(jnp.bfloat16)
    )
    return (cache_out, first_read)


def solution(mesh):
    placed = (
        P("grp", "sp", None),
        P("sp", "tp"),
        P("sp", "tp"),
        P("tp"),
        P("grp", "sp", "tp"),
        P("grp", "tp"),
        P("tp"),
    )
    return jax.shard_map(
        shards,
        mesh=mesh,
        in_specs=placed,
        out_specs=(P("grp", "tp", "sp"), P("grp", "tp")),
        check_vma=False,
    )
```

profile of v0, /device:TPU:65, one launch (start us, length us, event | category | flops | bytes accessed | tf_op | source)
XLA Modules:
  0.0 240.3 jit_solution(561585214322564502)
XLA Ops:
  7.2 1.7 pad_maximum_fusion
  9.0 0.8 copy.26
  9.9 0.7 fusion.28
  10.6 115.3 %all-gather.2.cloned.1.call-done = bf16[4096,1024]{1,0:T(8,128)(2,1)} async-done(((bf16[128,1024]{1,0:T(8,128)(2,1)}), bf16[4096,1024]{1,0:T(8,128)(2,1)}) %all-gather.2.cloned.1.call-update) | async-done | bytes 8388624 | tf_op jit(solution)/shard_map/all_gather | solution.py:12
  125.9 7.0 %add_select_fusion = (f32[512,512]{0,1:T(8,128)S(1)}, f32[512,512]{1,0:T(8,128)S(1)}) fusion(f32[512]{0:T(512)S(1)} %get-tuple-element.6, f32[512]{0:T(512)S(1)} %get-tuple-element.4, bf16[512,4096]{1,0:T(8,128)(2,1)} %bitcast.46, bf16[4096,1024]{1,0:T(8,128)(2,1)} %all-gather.2.cloned.1.call-done), kind=kOutput, calls=%fused_computation.22 | convolution fusion | flops 2151940096 | bytes 10489856 | tf_op jit(solution)/shard_map/dot_general | solution.py:73
  132.9 0.4 reshape.64
  133.2 0.4 copy.27
  133.7 0.7 fusion.17
  134.4 0.8 broadcast_in_dim.20
  135.2 8.0 %all-to-all-start = ((f32[32,4,4,128]{3,2,1,0:T(4,128)}), f32[32,4,4,128]{3,2,1,0:T(4,128)S(1)}, u32[]{:S(2)}, u32[]{:S(2)}) async-start(f32[32,4,4,128]{3,2,1,0:T(4,128)} %broadcast_in_dim.20), calls=%async_computation | async-start | bytes 524288 | tf_op jit(solution)/shard_map/all_to_all | solution.py:21
  143.2 5.8 %fusion.8 = bf16[512,512]{0,1:T(8,128)(2,1)S(1)} fusion(bf16[512,4096]{1,0:T(8,128)(2,1)} %bitcast.47, bf16[4096,1024]{1,0:T(8,128)(2,1)} %all-gather.2.cloned.1.call-done), kind=kOutput, calls=%fused_computation.8 | convolution fusion | flops 2147745792 | bytes 8912896 | tf_op jit(solution)/shard_map/dot_general | solution.py:74
  149.1 0.9 reshape.66
  150.7 0.4 copy.28
  151.1 0.4 multiply_convert_fusion
  151.5 13.8 %all-to-all-done = f32[32,4,4,128]{3,2,1,0:T(4,128)S(1)} async-done(((f32[32,4,4,128]{3,2,1,0:T(4,128)}), f32[32,4,4,128]{3,2,1,0:T(4,128)S(1)}, u32[]{:S(2)}, u32[]{:S(2)}) %all-to-all-start) | async-done | bytes 262176 | tf_op jit(solution)/shard_map/all_to_all | solution.py:21
  165.6 0.6 fusion.7
  166.5 1.2 copy.41
  167.7 4.4 %all-to-all-start.1 = ((bf16[32,4,4,512]{3,2,1,0:T(4,128)(2,1)}), bf16[32,4,4,512]{3,2,1,0:T(4,128)(2,1)S(1)}, u32[]{:S(2)}, u32[]{:S(2)}) async-start(bf16[32,4,4,512]{3,2,1,0:T(4,128)(2,1)} %bitcast.45), calls=%async_computation.1 | async-start | bytes 1048576 | tf_op jit(solution)/shard_map/all_to_all | solution.py:53
  172.2 33.3 %all-to-all-done.1 = bf16[32,4,4,512]{3,2,1,0:T(4,128)(2,1)S(1)} async-done(((bf16[32,4,4,512]{3,2,1,0:T(4,128)(2,1)}), bf16[32,4,4,512]{3,2,1,0:T(4,128)(2,1)S(1)}, u32[]{:S(2)}, u32[]{:S(2)}) %all-to-all-start.1) | async-done | bytes 524320 | tf_op jit(solution)/shard_map/all_to_all | solution.py:53
  205.9 0.7 broadcast_in_dim.35
  206.6 4.5 %all-to-all-start.2 = ((f32[32,4,4,128]{3,2,1,0:T(4,128)}), f32[32,4,4,128]{3,2,1,0:T(4,128)S(1)}, u32[]{:S(2)}, u32[]{:S(2)}) async-start(f32[32,4,4,128]{3,2,1,0:T(4,128)} %broadcast_in_dim.35), calls=%async_computation.2 | async-start | bytes 524288 | tf_op jit(solution)/shard_map/all_to_all | solution.py:21
  211.1 0.6 convert_element_type.34
  211.8 20.8 %all-to-all-done.2 = f32[32,4,4,128]{3,2,1,0:T(4,128)S(1)} async-done(((f32[32,4,4,128]{3,2,1,0:T(4,128)}), f32[32,4,4,128]{3,2,1,0:T(4,128)S(1)}, u32[]{:S(2)}, u32[]{:S(2)}) %all-to-all-start.2) | async-done | bytes 262176 | tf_op jit(solution)/shard_map/all_to_all | solution.py:21
  232.8 0.6 fusion.24
  (30 shorter events, 2.0 us)
Async XLA Ops:
  7.2 118.7 %all-gather.2.cloned.1.call-start = ((), (), s32[]{:S(2)}) async-start(), calls=%async_computation.3 | async-start | bytes 8650752 | tf_op jit(solution)/shard_map/all_gather | solution.py:12
  135.2 30.1 %all-to-all-start = ((f32[32,4,4,128]{3,2,1,0:T(4,128)}), f32[32,4,4,128]{3,2,1,0:T(4,128)S(1)}, u32[]{:S(2)}, u32[]{:S(2)}) async-start(f32[32,4,4,128]{3,2,1,0:T(4,128)} %broadcast_in_dim.20), calls=%async_computation | async-start | bytes 524288 | tf_op jit(solution)/shard_map/all_to_all | solution.py:21
  151.1 14.5 %copy-start = (bf16[4,128,4,128]{1,0,3,2:T(4,128)(2,1)S(1)}, bf16[4,128,4,128]{1,0,3,2:T(4,128)(2,1)}, u32[]{:S(2)}) copy-start(bf16[4,128,4,128]{1,0,3,2:T(4,128)(2,1)} %reshape.66) | copy-start | bytes 1572868
  151.1 21.0 %copy-start.1 = (bf16[4,512]{1,0:T(4,128)(2,1)S(1)}, bf16[4,512]{1,0:T(4,128)(2,1)}, u32[]{:S(2)}) copy-start(bf16[4,512]{1,0:T(4,128)(2,1)} %param.12) | copy-start | bytes 12292
  151.5 81.3 %copy-start.2 = (f32[512]{0:T(512)S(1)}, f32[512]{0:T(512)}, u32[]{:S(2)}) copy-start(f32[512]{0:T(512)} %param.13) | copy-start | bytes 6148
  167.7 37.8 %all-to-all-start.1 = ((bf16[32,4,4,512]{3,2,1,0:T(4,128)(2,1)}), bf16[32,4,4,512]{3,2,1,0:T(4,128)(2,1)S(1)}, u32[]{:S(2)}, u32[]{:S(2)}) async-start(bf16[32,4,4,512]{3,2,1,0:T(4,128)(2,1)} %bitcast.45), calls=%async_computation.1 | async-start | bytes 1048576 | tf_op jit(solution)/shard_map/all_to_all | solution.py:53
  206.6 26.0 %all-to-all-start.2 = ((f32[32,4,4,128]{3,2,1,0:T(4,128)}), f32[32,4,4,128]{3,2,1,0:T(4,128)S(1)}, u32[]{:S(2)}, u32[]{:S(2)}) async-start(f32[32,4,4,128]{3,2,1,0:T(4,128)} %broadcast_in_dim.35), calls=%async_computation.2 | async-start | bytes 524288 | tf_op jit(solution)/shard_map/all_to_all | solution.py:21
Sparse Core Ops, SparseCore 0:
  10.1 115.6 all-gather.1
where the time goes:
time: 241 us; the launch traced here: 240 us
  waiting for transfers between devices  183 us (76%)
  starting transfers between devices  17 us (7%)
  between operations  14.3 us (6%)
  matrix products  13.4 us (6%)
  local copies, waits for them, and re-layouts  6.5 us (3%)
  other arithmetic  5.81 us (2%)
    all_gather x1, waiting for transfers between devices, side_by_side(): lax.all_gather(both, axis, axis=dim, tiled=True)  115 us
    all_to_all x2, waiting for transfers between devices, sent_to_all(): lax.all_to_all(jnp.broadcast_to(array[None], (count, *array.shape)), axis...  34.6 us
    all_to_all x1, waiting for transfers between devices, sent_and_summed(): lax.all_to_all(blocks, axis, split_axis=0, concat_axis=0, tiled=True)  33.3 us
    all_to_all x2, starting transfers between devices, sent_to_all(): lax.all_to_all(jnp.broadcast_to(array[None], (count, *array.shape)), axis...  12.6 us
    dot_general x1, matrix products, shards(): pre_gate = jnp.dot(tok_rows, pieces[0], preferred_element_type=jnp.float32)  6.97 us
    dot_general x1, matrix products, shards(): value_sum = jnp.dot(tok_rows, pieces[1], preferred_element_type=jnp.float32)  5.85 us
  transfers between devices with their start and end apart: 4, of which 4 were waited for; matrix products, arithmetic and copies ran while one was open for 4% of the time, Pallas kernels for 0%

commit v1 on v0

v1 whole, which is shorter than its diff:
```python
import functools

import jax
import jax.numpy as jnp
from jax import lax
from jax.experimental import pallas as pl
from jax.experimental.pallas import tpu as pltpu
from jax.sharding import PartitionSpec as P

DK = 128
DV = 128
F32 = jnp.float32
BF16 = jnp.bfloat16

LONE_ROWS = (32, 48)
PIECE_ROWS = (32, 16)
NT = (((1,), (1,)), ((), ()))


def split3(x):
    hi = x.astype(BF16)
    rest = x - hi.astype(F32)
    mid = rest.astype(BF16)
    lo = (rest - mid.astype(F32)).astype(BF16)
    return hi, mid, lo


def exact_dot(ones, x, dims):
    total = None
    for part in split3(x):
        term = lax.dot_general(ones, part, dims, preferred_element_type=F32)
        total = term if total is None else total + term
    return total


def kernel(
    nz,
    lone,
    piece,
    tok_hbm,
    wf_hbm,
    wv_hbm,
    lb_ref,
    shift_ref,
    q_ref,
    gain_ref,
    cache_ref,
    read_ref,
    tok,
    w,
    acc,
    amat,
    upper,
    shift_suf,
    tot,
    sib_tot,
    chip_tot,
    far_tot,
    suf_half,
    suf,
    rows16,
    dcol,
    qcol,
    dec_state,
    pay,
    sib_pay,
    comb,
    comb_b,
    far_state,
    rloc,
    rsib,
    rchip,
    far_read,
    rtot,
    local_sem,
    rs0,
    ss0,
    rs1,
    ss1,
    yr,
    ys,
    dr,
    ds,
    sib_r,
    sib_s,
    ft_r,
    ft_s,
    fs_r,
    fs_s,
    fr_r,
    fr_s,
):
    seqs, heads = cache_ref.shape[0], cache_ref.shape[1]
    span = DK
    shard = wf_hbm.shape[0]
    width = wf_hbm.shape[1]
    own = DK // (2 * nz)
    group = own * heads
    half = nz // 2
    sp = lax.axis_index("sp")
    z = sp // 2
    c = sp % 2
    grp = lax.axis_index("grp")
    gpar = grp % 2
    partner = {"grp": grp + 1 - 2 * gpar}
    sibling = {"sp": sp + 1 - 2 * c}

    def chip(zz):
        return {"sp": 2 * zz + c}

    def wrap(v):
        return lax.rem(v + 2 * nz, nz)

    pieces = [(shard - lone[p]) // piece[p] for p in (0, 1)]
    firsts = [(n + 1) // 2 for n in pieces]
    zrecv = (rs0, rs1)
    zsend = (ss0, ss1)

    def ring(p, way, k, j, sending):
        sign = -1 if way == 0 else 1
        at = k if sending else k + 1
        slot = wrap(z + sign * at)
        row = pl.multiple_of(c * shard + gpar * lone[p] + j * piece[p], 16)
        ref = w.at[p, slot, pl.ds(row, piece[p]), :]
        return pltpu.make_async_remote_copy(
            src_ref=ref,
            dst_ref=ref,
            send_sem=zsend[p].at[way, k, j],
            recv_sem=zrecv[p].at[way, k, j],
            device_id=chip(wrap(z - sign)),
            device_id_type=pl.DeviceIdType.MESH,
        )

    def in_last(p, way, j):
        return j < firsts[p] if way == 0 else j >= firsts[p]

    def lone_copy(p, rel, sending):
        side = gpar if sending else 1 - gpar
        row = pl.multiple_of(c * shard + side * (shard - lone[p]), 16)
        ref = w.at[p, wrap(z - rel), pl.ds(row, lone[p]), :]
        return pltpu.make_async_remote_copy(
            src_ref=ref,
            dst_ref=ref,
            send_sem=ys.at[p, rel],
            recv_sem=yr.at[p, rel],
            device_id=partner,
            device_id_type=pl.DeviceIdType.MESH,
        )

    def pair_copy(p, rel, sending):
        side = c if sending else 1 - c
        row = pl.multiple_of(side * shard, 16)
        ref = w.at[p, wrap(z - rel), pl.ds(row, shard), :]
        return pltpu.make_async_remote_copy(
            src_ref=ref,
            dst_ref=ref,
            send_sem=ds.at[p, rel],
            recv_sem=dr.at[p, rel],
            device_id=sibling,
            device_id_type=pl.DeviceIdType.MESH,
        )

    def sib_copy(i, src, dst):
        return pltpu.make_async_remote_copy(
            src_ref=src,
            dst_ref=dst,
            send_sem=sib_s.at[i],
            recv_sem=sib_r.at[i],
            device_id=sibling,
            device_id_type=pl.DeviceIdType.MESH,
        )

    def far_copy(src, dst, send, recv, dz, sign):
        return pltpu.make_async_remote_copy(
            src_ref=src,
            dst_ref=dst,
            send_sem=send.at[dz],
            recv_sem=recv.at[dz],
            device_id=chip(wrap(z + sign * dz)),
            device_id_type=pl.DeviceIdType.MESH,
        )

    own_rows = pl.ds(pl.multiple_of(c * shard, 16), shard)
    copies = (
        pltpu.make_async_copy(wf_hbm, w.at[0, z, own_rows, :], local_sem.at[0]),
        pltpu.make_async_copy(wv_hbm, w.at[1, z, own_rows, :], local_sem.at[1]),
        pltpu.make_async_copy(tok_hbm, tok, local_sem.at[2]),
    )
    for cp in copies:
        cp.start()
    barrier = pltpu.get_barrier_semaphore()
    for peer in (chip(wrap(z + 1)), chip(wrap(z - 1)), sibling, partner):
        pl.semaphore_signal(
            barrier, inc=1, device_id=peer, device_id_type=pl.DeviceIdType.MESH
        )
    copies[0].wait()
    pl.semaphore_wait(barrier, 4)

    def own_sends(p):
        for j in range(pieces[p]):
            for way in (0, 1):
                ring(p, way, 0, j, True).start()
        pair_copy(p, 0, True).start()

    own_sends(0)
    copies[1].wait()

    acc[...] = jnp.zeros(acc.shape, F32)
    r_i = lax.broadcasted_iota(jnp.int32, (span, span), 0)
    c_i = lax.broadcasted_iota(jnp.int32, (span, span), 1)
    upper[...] = jnp.where(c_i > r_i, 1.0, 0.0).astype(BF16)
    shift_suf[...] = exact_dot(upper[...], shift_ref[...], NT)

    nrow = 2 * nz * group

    def perm():
        r = lax.broadcasted_iota(jnp.int32, (nrow, DK), 0)
        k = lax.broadcasted_iota(jnp.int32, (nrow, DK), 1)
        side = r // (nz * group)
        inner = r % (nz * group)
        key = (inner // group) * (2 * own) + side * own + (inner % group) // heads
        return jnp.where(k == key, 1.0, 0.0).astype(BF16)

    def head_of_row(cols):
        r = lax.broadcasted_iota(jnp.int32, (nrow, cols), 0)
        return r % heads

    def columns(x16, out):
        spread = exact_dot(perm(), x16, NT)
        head = head_of_row(spread.shape[1])
        lane = lax.broadcasted_iota(jnp.int32, spread.shape, 1)
        for s in range(seqs):
            col = jnp.sum(
                jnp.where(lane == s * heads + head, spread, 0.0), axis=1, keepdims=True
            )
            out[s] = jnp.broadcast_to(col, (nrow, DV))

    query = q_ref[...].astype(F32)
    query = query * jax.nn.sigmoid(query)
    for s in range(seqs):
        for h in range(heads):
            rows16[s * heads + h : s * heads + h + 1, :] = query[
                s : s + 1, h * DK : (h + 1) * DK
            ]
    columns(rows16[...], qcol)
    copies[2].wait()

    def gate(s):
        rows = pl.ds(pl.multiple_of(s * span, span), span)
        pre = acc[0, rows, :]
        key_gate = (1.0 - lb_ref[...]) * jax.nn.sigmoid(-pre)
        log_forget = jnp.log1p(-key_gate)
        later = exact_dot(upper[...], log_forget, (((1,), (0,)), ((), ())))
        total = jnp.sum(log_forget, axis=0, keepdims=True)
        lane = lax.broadcasted_iota(jnp.int32, shift_suf.shape, 1)
        head = head_of_row(span)
        for h in range(heads):
            cols = slice(h * DK, (h + 1) * DK)
            idx = s * heads + h
            shift = jnp.sum(
                jnp.where(lane == idx, shift_suf[...], 0.0), axis=1, keepdims=True
            )
            weighted = (key_gate[:, cols] * jnp.exp(later[:, cols] + shift)).astype(BF16)
            turned = lax.dot_general(perm(), weighted, NT, preferred_element_type=F32)
            amat[s, :, cols] = jnp.where(head == h, turned, 0.0).astype(BF16)
            tot[pl.ds(idx, 1), :] = total[:, cols] + jnp.sum(
                shift_ref[pl.ds(idx, 1), :], axis=1, keepdims=True
            )

    rows_half = seqs * heads // 2
    mine = pl.ds(pl.multiple_of(c * rows_half, 8), rows_half)
    theirs = pl.ds(pl.multiple_of((1 - c) * rows_half, 8), rows_half)
    tot_copy = sib_copy(0, tot, sib_tot)

    def send_totals():
        chip_tot[...] = tot[...] + sib_tot[...]

        @pl.loop(1, nz)
        def _(dz):
            @pl.when(z >= dz)
            def _():
                far_copy(chip_tot.at[mine, :], far_tot.at[z], ft_s, ft_r, dz, -1).start()

    suf_copy = sib_copy(1, suf_half.at[mine, :], suf_half.at[mine, :])
    suf_wait = sib_copy(1, suf_half.at[theirs, :], suf_half.at[theirs, :])

    def take_totals():
        suf_half[mine, :] = jnp.zeros((rows_half, DK), F32)

        @pl.loop(1, nz)
        def _(dz):
            @pl.when(z + dz < nz)
            def _():
                far_copy(
                    chip_tot.at[mine, :], far_tot.at[wrap(z + dz)], ft_s, ft_r, dz, -1
                ).wait_recv()
                suf_half[mine, :] += far_tot[wrap(z + dz)]

        suf_copy.start()

    def finish_suffix():
        suf_wait.wait_recv()
        suf[...] = jnp.exp(
            suf_half[...] + jnp.where(c == 0, 1.0, 0.0) * sib_tot[...]
        )
        columns(suf[...], dcol)

    def stage1(p, s):
        for j in range(pieces[p]):
            for way in (0, 1):

                @pl.when(jnp.logical_or(s < half, in_last(p, way, j)))
                def _():
                    ring(p, way, s - 1, j, False).wait_recv()

                @pl.when(
                    jnp.logical_or(
                        s < half - 1, jnp.logical_and(s == half - 1, in_last(p, way, j))
                    )
                )
                def _():
                    ring(p, way, s, j, True).start()

        if lone[p]:
            lone_copy(p, s, True).start()

            @pl.when(s < half)
            def _():
                lone_copy(p, nz - s, True).start()

    def stage2(p, s):
        if lone[p]:
            lone_copy(p, s, False).wait_recv()
        pair_copy(p, s, True).start()

        @pl.when(s < half)
        def _():
            if lone[p]:
                lone_copy(p, nz - s, False).wait_recv()
            pair_copy(p, nz - s, True).start()

    def multiply(p, rel):
        pair_copy(p, rel, False).wait_recv()
        slot = wrap(z - rel)
        cols = pl.ds(pl.multiple_of(slot * 2 * shard, 2 * shard), 2 * shard)
        acc[p] += jnp.dot(tok[:, cols], w[p, slot], preferred_element_type=F32)

    gate_at = half + 2
    pairs = seqs // 2
    last = 2 * half + 3

    @pl.loop(0, last)
    def _(t):
        @pl.when(t == half)
        def _():
            own_sends(1)

        for p in (0, 1):
            s = t - p * half

            @pl.when(jnp.logical_and(s >= 1, s <= half))
            def _():
                stage1(p, s)

            @pl.when(jnp.logical_and(s >= 2, s <= half + 1))
            def _():
                stage2(p, s - 1)

        @pl.loop(0, 4)
        def _(item):
            p = item // 2
            way = item % 2
            s = t - p * half - 2
            ok = jnp.logical_and(s >= 0, s <= half)
            ok = jnp.logical_and(
                ok, jnp.logical_or(way == 0, jnp.logical_and(s >= 1, s < half))
            )

            @pl.when(ok)
            def _():
                multiply(p, jnp.where(way == 0, s, nz - s))

        @pl.when(jnp.logical_and(t >= gate_at, t < gate_at + 2))
        def _():
            @pl.loop(0, pairs)
            def _(i):
                gate((t - gate_at) * pairs + i)

        @pl.when(t == gate_at + 1)
        def _():
            tot_copy.start()

        @pl.when(t == gate_at + 2)
        def _():
            tot_copy.wait_recv()
            send_totals()

        @pl.when(t == last - 2)
        def _():
            take_totals()

        @pl.when(t == last - 1)
        def _():
            finish_suffix()

    for s in range(seqs):
        rows = slice(s * span, (s + 1) * span)
        values = jnp.concatenate(
            [
                acc[1, rows, h * DV : (h + 1) * DV].astype(BF16)
                for h in range(heads)
            ],
            axis=0,
        )
        state = jnp.dot(amat[s], values, preferred_element_type=F32) * dcol[s]
        part = state.reshape(2, nz, group, DV)
        dec_state[:, :, s * group : (s + 1) * group, :] = part
        pay[:, :, s * group : (s + 1) * group, :] = part.astype(BF16)
        read = jnp.sum((state * qcol[s]).reshape(nrow // 8, 8, DV), axis=0)
        for h in range(heads):
            row = read[h : h + 1]
            for again in range(h + heads, 8, heads):
                row = row + read[again : again + 1]
            rloc[s * heads + h : s * heads + h + 1, :] = row

    state_copy = sib_copy(2, pay.at[1 - c], sib_pay)
    read_copy = sib_copy(3, rloc, rsib)
    state_copy.start()
    read_copy.start()
    read_copy.wait_recv()
    rchip[...] = rloc[...] + rsib[...]
    state_copy.wait_recv()
    comb[...] = dec_state[c] + sib_pay[...].astype(F32)
    comb_b[...] = comb[...].astype(BF16)

    @pl.loop(1, nz)
    def _(dz):
        far_copy(comb_b.at[wrap(z + dz)], far_state.at[z], fs_s, fs_r, dz, 1).start()
        far_copy(rchip.at[mine, :], far_read.at[z], fr_s, fr_r, dz, 1).start()

    rtot[mine, :] = rchip[mine, :]
    comb[0] = comb[z]

    @pl.loop(1, nz)
    def _(dz):
        src = wrap(z - dz)
        far_copy(rchip.at[mine, :], far_read.at[src], fr_s, fr_r, dz, 1).wait_recv()
        rtot[mine, :] += far_read[src]

    final_copy = sib_copy(4, rtot.at[mine, :], rtot.at[mine, :])
    final_wait = sib_copy(4, rtot.at[theirs, :], rtot.at[theirs, :])
    final_copy.start()

    @pl.loop(1, nz)
    def _(dz):
        src = wrap(z - dz)
        far_copy(comb_b.at[0], far_state.at[src], fs_s, fs_r, dz, 1).wait_recv()
        comb[0] += far_state[src].astype(F32)

    final = comb[0]
    for s in range(seqs):
        for i in range(own):
            at = s * group + i * heads
            cache_ref[s, :, i * DV : (i + 1) * DV] = final[at : at + heads].astype(BF16)

    final_wait.wait_recv()
    total = rtot[...]
    scaled = total * lax.rsqrt(jnp.mean(total * total, axis=-1, keepdims=True) + 1e-06)
    for s in range(seqs):
        for h in range(heads):
            cols = slice(h * DV, (h + 1) * DV)
            at = s * heads + h
            read_ref[s : s + 1, cols] = (scaled[at : at + 1] * gain_ref[:, cols]).astype(BF16)

    for p in (0, 1):

        @pl.loop(0, half)
        def _(k):
            for way in (0, 1):
                for j in range(pieces[p]):

                    @pl.when(jnp.logical_or(k < half - 1, in_last(p, way, j)))
                    def _():
                        ring(p, way, k, j, True).wait_send()

        @pl.loop(0, nz)
        def _(rel):
            pair_copy(p, rel, True).wait_send()
            if lone[p]:

                @pl.when(rel >= 1)
                def _():
                    lone_copy(p, rel, True).wait_send()

    for cp in (tot_copy, suf_copy, state_copy, read_copy, final_copy):
        cp.wait_send()

    @pl.loop(1, nz)
    def _(dz):
        @pl.when(z >= dz)
        def _():
            far_copy(chip_tot.at[mine, :], far_tot.at[z], ft_s, ft_r, dz, -1).wait_send()

        far_copy(comb_b.at[wrap(z + dz)], far_state.at[z], fs_s, fs_r, dz, 1).wait_send()
        far_copy(rchip.at[mine, :], far_read.at[z], fr_s, fr_r, dz, 1).wait_send()


def shards(tokens, w_forget, w_value, lower_bound, decay_shift, queries, read_gain):
    seqs, span, feat = tokens.shape
    shard, width = w_forget.shape
    heads = width // DK
    nz = lax.axis_size("sp") // 2
    half = nz // 2
    own = DK // (2 * nz)
    group = own * heads
    nrow = 2 * nz * group
    n = seqs * heads
    lone = LONE_ROWS if lax.axis_size("grp") % 2 == 0 else (0, 0)
    pieces = [(shard - lone[p]) // PIECE_ROWS[p] for p in (0, 1)]
    dma = pltpu.SemaphoreType.DMA
    vmem = pl.BlockSpec(memory_space=pltpu.VMEM)
    anywhere = pl.BlockSpec(memory_space=pl.ANY)
    cache_out, first_read = pl.pallas_call(
        functools.partial(kernel, nz, lone, PIECE_ROWS),
        out_shape=(
            jax.ShapeDtypeStruct((seqs, heads, own * DV), BF16),
            jax.ShapeDtypeStruct((seqs, heads * DV), BF16),
        ),
        in_specs=[anywhere] * 3 + [vmem] * 4,
        out_specs=(vmem, vmem),
        scratch_shapes=[
            pltpu.VMEM((seqs * span, feat), BF16),
            pltpu.VMEM((2, nz, 2 * shard, width), BF16),
            pltpu.VMEM((2, seqs * span, width), F32),
            pltpu.VMEM((seqs, nrow, heads * span), BF16),
            pltpu.VMEM((span, span), BF16),
            pltpu.VMEM((span, n), F32),
            pltpu.VMEM((n, DK), F32),
            pltpu.VMEM((n, DK), F32),
            pltpu.VMEM((n, DK), F32),
            pltpu.VMEM((nz, n // 2, DK), F32),
            pltpu.VMEM((n, DK), F32),
            pltpu.VMEM((n, DK), F32),
            pltpu.VMEM((n, DK), F32),
            pltpu.VMEM((seqs, nrow, DV), F32),
            pltpu.VMEM((seqs, nrow, DV), F32),
            pltpu.VMEM((2, nz, seqs * group, DV), F32),
            pltpu.VMEM((2, nz, seqs * group, DV), BF16),
            pltpu.VMEM((nz, seqs * group, DV), BF16),
            pltpu.VMEM((nz, seqs * group, DV), F32),
            pltpu.VMEM((nz, seqs * group, DV), BF16),
            pltpu.VMEM((nz, seqs * group, DV), BF16),
            pltpu.VMEM((n, DV), F32),
            pltpu.VMEM((n, DV), F32),
            pltpu.VMEM((n, DV), F32),
            pltpu.VMEM((nz, n // 2, DV), F32),
            pltpu.VMEM((n, DV), F32),
            dma((3,)),
            dma((2, half, pieces[0])),
            dma((2, half, pieces[0])),
            dma((2, half, pieces[1])),
            dma((2, half, pieces[1])),
            dma((2, nz)),
            dma((2, nz)),
            dma((2, nz)),
            dma((2, nz)),
            dma((5,)),
            dma((5,)),
            dma((nz,)),
            dma((nz,)),
            dma((nz,)),
            dma((nz,)),
            dma((nz,)),
            dma((nz,)),
        ],
        compiler_params=pltpu.CompilerParams(
            collective_id=0, has_side_effects=True, vmem_limit_bytes=48 * 1024 * 1024
        ),
    )(
        tokens.reshape(seqs * span, feat),
        w_forget,
        w_value,
        lower_bound.reshape(1, width),
        decay_shift.transpose(0, 2, 1).reshape(n, span),
        queries,
        read_gain.reshape(1, heads * DV),
    )
    return cache_out, first_read


def solution(mesh):
    placed = (
        P("grp", "sp", None),
        P("sp", "tp"),
        P("sp", "tp"),
        P("tp"),
        P("grp", "sp", "tp"),
        P("grp", "tp"),
        P("tp"),
    )
    return jax.shard_map(
        shards,
        mesh=mesh,
        in_specs=placed,
        out_specs=(P("grp", "tp", "sp"), P("grp", "tp")),
        check_vma=False,
    )
```

time: 241 us -> 141 us (0.59)
  waiting for transfers between devices: 183 us -> 0 us
  Pallas kernels: 0 us -> 132 us
  starting transfers between devices: 17 us -> 0 us
  between operations: 14.3 us -> 0.66 us
  matrix products: 13.4 us -> 0 us
  other arithmetic: 5.81 us -> 0 us
    pallas_call x0 -> x1, Pallas kernels: none -> 132 us  [shards(): pl.pallas_call(functools.partial(kernel, nz, lone, PIECE_ROWS), out_shape...]
    all_gather x1 -> x0, waiting for transfers between devices: 115 us -> none  [side_by_side(): lax.all_gather(both, axis, axis=dim, tiled=True)]
    all_to_all x3 -> x0, waiting for transfers between devices: 67.9 us -> none  [the longest x2 34.6 us: sent_to_all(): lax.all_to_all(jnp.broadcast_to(array[None], (count, *array.shape)), axis...]
    all_to_all x3 -> x0, starting transfers between devices: 16.9 us -> none  [the longest x2 12.6 us: sent_to_all(): lax.all_to_all(jnp.broadcast_to(array[None], (count, *array.shape)), axis...]
    dot_general x3 -> x0, matrix products: 13.4 us -> none  [the longest x1 6.97 us: shards(): pre_gate = jnp.dot(tok_rows, pieces[0], preferred_element_type=jnp.float32)]
    unnamed x7 -> x16, local copies, waits for them, and re-layouts: 0.85 us -> 7.93 us
    reshape x7 -> x0, local copies, waits for them, and re-layouts: 2.53 us -> none  [the longest x1 0.91 us: shards(): span_values = values.reshape(seq_count, span_len, head_local, DV)]
  transfers between devices with their start and end apart: 4 -> 0, of which waited for: 4 -> 0; matrix products, arithmetic and copies ran while one was open for 4% -> 0% of each run, Pallas kernels for 0% -> 0%
where the time goes in v1:
time: 141 us; the launch traced here: 140 us
  Pallas kernels  132 us (94%)
  local copies, waits for them, and re-layouts  7.93 us (6%)
    pallas_call x1, Pallas kernels, shards(): pl.pallas_call(functools.partial(kernel, nz, lone, PIECE_ROWS), out_shape...  132 us
    unnamed x16, local copies, waits for them, and re-layouts  7.93 us

profile of v1, /device:TPU:65, one launch (start us, length us, event | category | flops | bytes accessed | tf_op | source)
XLA Modules:
  0.0 140.5 jit_solution(14818313828701487771)
XLA Ops:
  0.6 0.0 copy-start
  0.6 2.2 %copy-done = bf16[4,128,4096]{2,1,0:T(8,128)(2,1)S(1)} copy-done((bf16[4,128,4096]{2,1,0:T(8,128)(2,1)S(1)}, bf16[4,128,4096]{2,1,0:T(8,128)(2,1)}, u32[]{:S(2)}) %copy-start) | copy-done | bytes 4194328
  2.8 0.0 copy-start.1
  2.8 0.9 copy-done.1
  3.7 0.0 copy-start.2
  3.7 0.9 copy-done.2
  4.6 0.0 copy-start.3
  4.6 0.7 copy-done.3
  5.3 0.0 copy-start.4
  5.3 0.7 copy-done.4
  6.0 0.0 copy-start.5
  6.0 0.7 copy-done.5
  6.7 0.0 copy-start.6
  6.7 0.7 copy-done.6
  7.4 131.9 %shard_map.86 = (bf16[4,4,512]{2,1,0:T(4,128)(2,1)S(1)}, bf16[4,512]{1,0:T(4,128)(2,1)S(1)}) custom-call(bf16[512,4096]{1,0:T(8,128)(2,1)S(1)} %bitcast.6, bf16[128,512]{1,0:T(8,128)(2,1)S(1)} %copy-done.1, bf16[128,512]{1,0:T(8,128)(2,1)S(1)} %copy-done.2, f32[1,512]{1,0:T(1,128)S(1)} %bitcast.8, f32[16,128]{1,0:T(8,128)S(1)} %bitcast.7, ...), custom_call_target="tpu_custom_call" | custom-call | tf_op jit(solution)/shard_map/pallas_call | solution.py:523
  139.3 0.6 copy.11
  139.9 0.6 copy.12
Async XLA Ops:
  0.6 2.2 %copy-start = (bf16[4,128,4096]{2,1,0:T(8,128)(2,1)S(1)}, bf16[4,128,4096]{2,1,0:T(8,128)(2,1)}, u32[]{:S(2)}) copy-start(bf16[4,128,4096]{2,1,0:T(8,128)(2,1)} %param.7) | copy-start | bytes 12582916
  2.8 0.9 copy-start.1
  3.7 0.9 copy-start.2
  4.6 0.7 copy-start.3
  5.3 0.7 copy-start.4
  6.0 0.7 copy-start.5
  6.7 0.7 copy-start.6
